TPU v7x, 256 devices: a whole 4x4x8 slice. The times are simulated.
256 devices in a mesh: sp: 32 (over z, y), dp: 8 (over x, core).
Axes of the slice: x: 4, y: 4, z: 8, core: 2. Of those that a mesh axis runs over, the one named last changes fastest.
Arguments:
- cotangent: bfloat16 [8, 8192, 4096], P('dp', 'sp'), may hold values from -6 to 6
- up_pre: bfloat16 [8, 8192, 4096], P('dp', 'sp'), may hold values from -6 to 6
- value_pre: bfloat16 [8, 8192, 4096], P('dp', 'sp'), may hold values from -6 to 6
- spatial_weight: bfloat16 [32, 1024, 1024], P('sp', 'dp'), may hold values from -0.1875 to 0.1875
- spatial_bias: float32 [32, 1024], P('sp'), may hold values from 0.5 to 1.5
- value_gain: float32 [4096], replicated, may hold values from 0.1 to 1.9
Outputs:
- up_grad: bfloat16 [8, 8192, 4096], P('dp', 'sp')
- value_grad: bfloat16 [8, 8192, 4096], P('dp', 'sp')
- weight_grad: float32 [32, 1024, 1024], P('sp', 'dp')
- bias_grad: float32 [32, 1024], P('sp', 'dp')
- gain_grad: float32 [4096], replicated
All inputs are finite; a program needn't handle non-finite values.
Results may differ from a plain program's by a relative error of at most 0.0064.
Values may be sent and summed in bfloat16 or wider, within the bound.
A program may use at most 128 MiB of HBM per device.

v0:
```python
import math
import jax
import jax.numpy as jnp
from jax import lax
from jax.sharding import Mesh
from jax.sharding import PartitionSpec as P

SP = ("sp_0", "sp_1")
DP = ("dp_0", "dp_1")
PLANE = ("dp_0", "dp_1", "sp_1")
SWAP = ("sp_0", "dp_0", "dp_1")
ALL = ("sp_0", "sp_1", "dp_0", "dp_1")
norm_floor = 0.5
root_half = 1.0 / math.sqrt(2.0)
inv_root_tau = 1.0 / math.sqrt(2.0 * math.pi)


def gelu_slope(values):
    return (
        0.5 * (1.0 + jax.scipy.special.erf(values * root_half))
        + values * jnp.exp(-0.5 * values * values) * inv_root_tau
    )


def swapped(shard, n):
    pairs = [(a * n + b, b * n + a) for a in range(n) for b in range(n)]
    return lax.ppermute(shard, SWAP, pairs)


def shards(cotangent, up_pre, value_pre, spatial_weight, spatial_bias, value_gain):
    rows, width = cotangent.shape[1:]
    block_len = spatial_weight.shape[2]
    planes = lax.axis_size("sp_0")
    seqs = lax.axis_size(DP)
    groups = lax.axis_size(PLANE)
    dim = width // groups
    weight = lax.all_gather(swapped(spatial_weight[0], planes), "sp_0", axis=0, tiled=True)
    bias = swapped(spatial_bias, planes)[0]
    grad_tok = cotangent[0].astype(jnp.float32)
    up_arg = up_pre[0].astype(jnp.float32)
    value_arg = value_pre[0].astype(jnp.float32)
    up_act = lax.optimization_barrier(jax.nn.gelu(up_arg, approximate=False).astype(jnp.bfloat16))
    value_act = jax.nn.gelu(value_arg, approximate=False)
    inv_rms = lax.rsqrt(jnp.mean(value_act * value_act, axis=-1, keepdims=True) + norm_floor)
    normed = value_act * inv_rms
    value_norm = (normed * value_gain).astype(jnp.bfloat16)
    gate_tok = (grad_tok * up_act.astype(jnp.float32)).astype(jnp.bfloat16)

    def outward(tok):
        tok = tok.reshape(rows, groups, dim).transpose(1, 0, 2)
        got = lax.all_to_all(tok, PLANE, split_axis=0, concat_axis=0, tiled=True)
        return got.reshape(seqs, block_len, dim)

    def homeward(heads):
        got = heads.reshape(groups, rows, dim)
        got = lax.all_to_all(got, PLANE, split_axis=0, concat_axis=0, tiled=True)
        return got.transpose(1, 0, 2).reshape(rows, width)

    value_blocks = outward(value_norm)
    gate_blocks = outward(gate_tok)
    back_heads = jnp.einsum(
        "pq,npc->nqc", weight, gate_blocks, preferred_element_type=jnp.float32
    ).astype(jnp.bfloat16)
    back_full = homeward(back_heads).astype(jnp.float32)
    mixed_heads = jnp.einsum(
        "pq,nqc->npc", weight, value_blocks, preferred_element_type=jnp.float32
    )
    mixed_heads = (mixed_heads + bias[None, :, None]).astype(jnp.bfloat16)
    mixed_tok = homeward(mixed_heads).astype(jnp.float32)
    weight_term = jnp.einsum(
        "npc,nqc->pq", gate_blocks, value_blocks, preferred_element_type=jnp.float32
    )
    bias_term = jnp.sum(gate_blocks, axis=(0, 2), dtype=jnp.float32)
    both = jnp.concatenate(
        [weight_term, jnp.broadcast_to(bias_term[:, None], (block_len, 128))], axis=1
    )
    both = lax.psum_scatter(both, "sp_0", scatter_dimension=0, tiled=True)
    both = swapped(both, planes)
    weight_grad = both[None, :, :block_len]
    bias_grad = both[None, :, block_len]
    up_mid = lax.optimization_barrier((grad_tok * mixed_tok).astype(jnp.bfloat16))
    up_grad = (up_mid.astype(jnp.float32) * gelu_slope(up_arg)).astype(jnp.bfloat16)[None]
    gain_grad = lax.psum(jnp.sum(back_full * normed, axis=0), ALL)
    scaled = back_full * value_gain
    value_slope = inv_rms * scaled - inv_rms**3 * value_act * jnp.mean(
        scaled * value_act, axis=-1, keepdims=True
    )
    value_grad = (value_slope * gelu_slope(value_arg)).astype(jnp.bfloat16)[None]
    return (up_grad, value_grad, weight_grad, bias_grad, gain_grad)


def solution(mesh):
    torus = Mesh(mesh.devices.reshape(8, 4, 4, 2), ("sp_0", "sp_1", "dp_0", "dp_1"))
    in_specs = (
        P(DP, SP, None),
        P(DP, SP, None),
        P(DP, SP, None),
        P(SP, DP, None),
        P(SP, None),
        P(),
    )
    out_specs = (P(DP, SP, None), P(DP, SP, None), P(SP, DP, None), P(SP, DP), P())
    return jax.shard_map(
        shards, mesh=torus, in_specs=in_specs, out_specs=out_specs, check_vma=False
    )
```

profile of v0, /device:TPU:47, one launch (start us, length us, event | category | flops | bytes accessed | tf_op | source)
XLA Modules:
  0.0 385.7 jit_solution(6176144169898661657)
XLA Ops:
  7.2 6.9 %collective-permute-start = (bf16[128,1024]{1,0:T(8,128)(2,1)}, bf16[128,1024]{1,0:T(8,128)(2,1)S(1)}, u32[]{:S(2)}, u32[]{:S(2)}) collective-permute-start(bf16[128,1024]{1,0:T(8,128)(2,1)} %bitcast.165), channel_id=1, source_target_pairs={{0,0},{1,32},{2,64},{3,96},{4,128},{5,160},{6,192},{7,224},{32,1},... | collective-permute-start | bytes 786440 | tf_op jit(solution)/shard_map/ppermute | solution.py:27
  17.5 15.1 %collective-permute-done = bf16[128,1024]{1,0:T(8,128)(2,1)S(1)} collective-permute-done((bf16[128,1024]{1,0:T(8,128)(2,1)}, bf16[128,1024]{1,0:T(8,128)(2,1)S(1)}, u32[]{:S(2)}, u32[]{:S(2)}) %collective-permute-start) | collective-permute-done | bytes 262176 | tf_op jit(solution)/shard_map/ppermute | solution.py:27
  33.3 10.0 %fusion.10 = bf16[256,4096]{0,1:T(8,128)(2,1)} fusion(bf16[1,256,4096]{1,2,0:T(8,128)(2,1)S(1)} %copy.39), kind=kLoop, calls=%fused_computation.29 | loop fusion | flops 69206016 | bytes 4194304 | tf_op jit(solution)/shard_map/convert_element_type | solution.py:42
  43.3 4.1 %copy.33 = bf16[1,256,4096]{1,2,0:T(8,128)(2,1)} copy(bf16[1,256,4096]{2,1,0:T(8,128)(2,1)} %param.6) | data formatting | bytes 4194304 | tf_op args[0]
  47.4 4.1 %fusion.1 = bf16[256,4096]{0,1:T(8,128)(2,1)} fusion(bf16[256,4096]{0,1:T(8,128)(2,1)} %fusion.10, bf16[1,256,4096]{1,2,0:T(8,128)(2,1)} %copy.33), kind=kLoop, calls=%fused_computation.20 | loop fusion | flops 4194304 | bytes 6291456 | tf_op jit(solution)/shard_map/convert_element_type | solution.py:47
  51.5 7.0 %all-to-all-start.2 = ((bf16[32,256,128]{1,2,0:T(8,128)(2,1)}), bf16[32,256,128]{1,2,0:T(8,128)(2,1)}, u32[]{:S(2)}, u32[]{:S(2)}) async-start(bf16[32,256,128]{1,2,0:T(8,128)(2,1)} %bitcast.155), calls=%async_computation.2 | async-start | bytes 4194304 | tf_op jit(solution)/shard_map/all_to_all | solution.py:51
  61.9 22.7 %all-to-all-done.2 = bf16[32,256,128]{1,2,0:T(8,128)(2,1)} async-done(((bf16[32,256,128]{1,2,0:T(8,128)(2,1)}), bf16[32,256,128]{1,2,0:T(8,128)(2,1)}, u32[]{:S(2)}, u32[]{:S(2)}) %all-to-all-start.2) | async-done | bytes 2097184 | tf_op jit(solution)/shard_map/all_to_all | solution.py:51
  84.5 4.1 %copy.40 = bf16[32,256,128]{2,1,0:T(8,128)(2,1)} copy(bf16[32,256,128]{1,2,0:T(8,128)(2,1)} %all-to-all-done.2) | data formatting | bytes 4194304 | tf_op jit(solution)/shard_map/all_to_all | solution.py:51
  88.6 6.0 %convert_bitcast_fusion.1 = bf16[8,1024,128]{1,2,0:T(8,128)(2,1)} fusion(bf16[8,1024,128]{2,1,0:T(8,128)(2,1)} %bitcast.158, bf16[1024,1024]{1,0:T(8,128)(2,1)} %all-gather.2.cloned.1.call-done), kind=kOutput, calls=%fused_computation.165 | convolution fusion | flops 2148532224 | bytes 6291456 | tf_op jit(solution)/shard_map/pq,npc->nqc/dot_general | solution.py:61
  94.5 3.9 %copy.42 = bf16[8,1024,128]{2,1,0:T(8,128)(2,1)} copy(bf16[8,1024,128]{1,2,0:T(8,128)(2,1)} %convert_bitcast_fusion.1) | data formatting | bytes 4194304 | tf_op jit(solution)/shard_map/convert_element_type | solution.py:63
  98.5 4.1 %copy.43 = bf16[32,256,128]{1,2,0:T(8,128)(2,1)} copy(bf16[32,256,128]{2,1,0:T(8,128)(2,1)} %bitcast.157) | data formatting | bytes 4194304 | tf_op jit(solution)/shard_map/reshape | solution.py:55
  102.5 7.5 %all-to-all-start.3 = ((bf16[32,256,128]{1,2,0:T(8,128)(2,1)}), bf16[32,256,128]{1,2,0:T(8,128)(2,1)}, u32[]{:S(2)}, u32[]{:S(2)}) async-start(bf16[32,256,128]{1,2,0:T(8,128)(2,1)} %copy.43), calls=%async_computation.3 | async-start | bytes 4194304 | tf_op jit(solution)/shard_map/all_to_all | solution.py:56
  110.0 9.4 %fusion.7 = f32[256]{0:T(256)S(1)} fusion(bf16[1,256,4096]{1,2,0:T(8,128)(2,1)S(1)} %copy.34), kind=kLoop, calls=%fused_computation.26 | loop fusion | flops 70254336 | bytes 2098176 | tf_op jit(solution)/shard_map/reduce_sum | solution.py:44
  123.2 12.8 %all-to-all-done.3 = bf16[32,256,128]{1,2,0:T(8,128)(2,1)} async-done(((bf16[32,256,128]{1,2,0:T(8,128)(2,1)}), bf16[32,256,128]{1,2,0:T(8,128)(2,1)}, u32[]{:S(2)}, u32[]{:S(2)}) %all-to-all-start.3) | async-done | bytes 2097184 | tf_op jit(solution)/shard_map/all_to_all | solution.py:56
  136.0 11.6 %fusion.61 = (f32[32,128]{1,0:T(8,128)S(1)}, f32[256]{0:T(256)S(1)}, f32[256,32,128]{0,2,1:T(8,128)S(1)}) fusion(bf16[32,256,128]{1,2,0:T(8,128)(2,1)} %all-to-all-done.3, f32[256]{0:T(256)S(1)} %get-tuple-element.31, f32[32,128]{1,0:T(8,128)S(1)} %bitcast.162, f32[256,32,128]{0,2,1:T(8,128)} %bitcast.154, f32[256,32,128]{0,2,1:T(8,128)} %bitcast.153), kind=kLoop, calls=%fused_computation.83 | loop fusion | flops 71298816 | bytes 14714880 | tf_op jit(solution)/shard_map/reduce_sum | solution.py:83
  149.3 7.5 %all-to-all-start = ((bf16[32,256,128]{1,2,0:T(8,128)(2,1)}), bf16[32,256,128]{1,2,0:T(8,128)(2,1)}, u32[]{:S(2)}, u32[]{:S(2)}) async-start(bf16[32,256,128]{1,2,0:T(8,128)(2,1)} %fusion.121), calls=%async_computation | async-start | bytes 4194304 | tf_op jit(solution)/shard_map/all_to_all | solution.py:51
  159.0 23.7 %all-to-all-done = bf16[32,256,128]{1,2,0:T(8,128)(2,1)} async-done(((bf16[32,256,128]{1,2,0:T(8,128)(2,1)}), bf16[32,256,128]{1,2,0:T(8,128)(2,1)}, u32[]{:S(2)}, u32[]{:S(2)}) %all-to-all-start) | async-done | bytes 2097184 | tf_op jit(solution)/shard_map/all_to_all | solution.py:51
  182.7 4.1 %copy.35 = bf16[32,256,128]{2,1,0:T(8,128)(2,1)} copy(bf16[32,256,128]{1,2,0:T(8,128)(2,1)} %all-to-all-done) | data formatting | bytes 4194304 | tf_op jit(solution)/shard_map/all_to_all | solution.py:51
  186.8 4.6 %convolution_bitcast_fusion = f32[1024,1024]{0,1:T(8,128)S(1)} fusion(bf16[8,1024,128]{2,1,0:T(8,128)(2,1)} %bitcast.159, bf16[8,1024,128]{2,1,0:T(8,128)(2,1)} %bitcast.160), kind=kOutput, calls=%fused_computation.158 | convolution fusion | flops 2147483648 | bytes 8388608 | tf_op jit(solution)/shard_map/npc,nqc->pq/dot_general | solution.py:70
  194.6 5.6 %collective-permute-start.1 = (f32[1,1024]{1,0:T(1,128)S(1)}, f32[1,1024]{1,0:T(1,128)S(1)}, u32[]{:S(2)}, u32[]{:S(2)}) collective-permute-start(f32[1,1024]{1,0:T(1,128)S(1)} %copy-done.6), channel_id=1, source_target_pairs={{0,0},{1,32},{2,64},{3,96},{4,128},{5,160},{6,192},{7,224},{32,1},... | collective-permute-start | bytes 12296 | tf_op jit(solution)/shard_map/ppermute | solution.py:27
  200.2 4.1 %convert_element_type.124 = f32[32,256,128]{1,2,0:T(8,128)} convert(bf16[32,256,128]{1,2,0:T(8,128)(2,1)} %all-to-all-done.3) | non-fusion elementwise | flops 1048576 | bytes 6291456 | tf_op jit(solution)/shard_map/convert_element_type | solution.py:64
  208.1 3.9 %copy.37 = bf16[8,1024,128]{2,1,0:T(8,128)(2,1)} copy(bf16[8,1024,128]{1,2,0:T(8,128)(2,1)} %fusion.122) | data formatting | bytes 4194304 | tf_op jit(solution)/shard_map/convert_element_type | solution.py:68
  212.0 8.6 %all-to-all-start.1 = ((bf16[32,256,128]{2,1,0:T(8,128)(2,1)}), bf16[32,256,128]{2,1,0:T(8,128)(2,1)}, u32[]{:S(2)}, u32[]{:S(2)}) async-start(bf16[32,256,128]{2,1,0:T(8,128)(2,1)} %bitcast.156), calls=%async_computation.1 | async-start | bytes 4194304 | tf_op jit(solution)/shard_map/all_to_all | solution.py:56
  220.6 15.5 %fusion.17 = bf16[1,256,4096]{1,2,0:T(8,128)(2,1)} fusion(bf16[1,256,4096]{1,2,0:T(8,128)(2,1)S(1)} %copy.34, f32[256]{0:T(256)S(1)} %broadcast_multiply_fusion, f32[256]{0:T(256)S(1)} %get-tuple-element.30, f32[4096]{0:T(1024)S(1)} %copy-done.4, f32[256]{0:T(256)S(1)} %get-tuple-element.31, f32[1,256,4096]{1,2,0:T(8,128)} %bitcast.152), kind=kLoop, calls=%fused_computation.36 | loop fusion | flops 83886080 | bytes 8408064 | tf_op jit(solution)/shard_map/convert_element_type | solution.py:88
  236.2 4.1 %copy.45 = bf16[1,256,4096]{2,1,0:T(8,128)(2,1)} copy(bf16[1,256,4096]{1,2,0:T(8,128)(2,1)} %fusion.17) | data formatting | bytes 4194304
  240.2 76.8 %psum.7 = f32[4096]{0:T(1024)} all-reduce(f32[4096]{0:T(1024)S(1)} %bitcast.164), channel_id=1, replica_groups=mesh['sp_0'=8,'sp_1'=4,'dp_0'=4,'dp_1'=2] {'sp_0','sp_1','dp_0','dp_1'}, use_global_device_ids=true, to_apply=%region_6.7 | all-reduce | flops 4096 | bytes 32768 | tf_op jit(solution)/shard_map/psum | solution.py:83
  317.0 4.1 %convert_bitcast_fusion = f32[256,32,128]{2,0,1:T(8,128)} fusion(bf16[32,256,128]{2,1,0:T(8,128)(2,1)} %all-to-all-done.1), kind=kLoop, calls=%fused_computation.140 | loop fusion | flops 1048576 | bytes 6291456 | tf_op jit(solution)/shard_map/convert_element_type | solution.py:69
  321.1 5.7 %copy.38 = f32[256,32,128]{0,2,1:T(8,128)} copy(f32[256,32,128]{2,0,1:T(8,128)} %convert_bitcast_fusion) | data formatting | bytes 8388608 | tf_op jit(solution)/shard_map/convert_element_type | solution.py:69
  326.8 4.8 %fusion = bf16[256,4096]{0,1:T(8,128)(2,1)} fusion(f32[256,32,128]{0,2,1:T(8,128)} %copy.38, bf16[1,256,4096]{1,2,0:T(8,128)(2,1)} %copy.33), kind=kLoop, calls=%fused_computation.19 | loop fusion | flops 3145728 | bytes 8388608 | tf_op jit(solution)/shard_map/convert_element_type | solution.py:81
  335.5 4.2 %fusion.127 = bf16[1,256,4096]{1,2,0:T(8,128)(2,1)} fusion(bf16[1,256,4096]{1,2,0:T(8,128)(2,1)S(1)} %copy-done.1, bf16[256,4096]{0,1:T(8,128)(2,1)} %fusion), kind=kLoop, calls=%fused_computation.166 | loop fusion | flops 12582912 | bytes 6291456 | tf_op jit(solution)/shard_map/broadcast_in_dim | solution.py:82
  339.7 4.1 %copy.44 = bf16[1,256,4096]{2,1,0:T(8,128)(2,1)} copy(bf16[1,256,4096]{1,2,0:T(8,128)(2,1)} %fusion.127) | data formatting | bytes 4194304
  343.8 33.5 %collective-permute-done.2 = f32[128,1152]{0,1:T(8,128)S(1)} collective-permute-done((f32[128,1152]{0,1:T(8,128)}, f32[128,1152]{0,1:T(8,128)S(1)}, u32[]{:S(2)}, u32[]{:S(2)}) %collective-permute-start.2) | collective-permute-done | bytes 589856 | tf_op jit(solution)/shard_map/ppermute | solution.py:27
  (38 shorter events, 27.4 us)
Async XLA Ops:
  7.2 81.4 %all-gather.2.cloned.1.call-start = ((), (), s32[]{:S(2)}) async-start(), calls=%async_computation.5 | async-start | bytes 2359296 | tf_op jit(solution)/shard_map/all_gather | solution.py:37
  7.2 25.4 %collective-permute-start = (bf16[128,1024]{1,0:T(8,128)(2,1)}, bf16[128,1024]{1,0:T(8,128)(2,1)S(1)}, u32[]{:S(2)}, u32[]{:S(2)}) collective-permute-start(bf16[128,1024]{1,0:T(8,128)(2,1)} %bitcast.165), channel_id=1, source_target_pairs={{0,0},{1,32},{2,64},{3,96},{4,128},{5,160},{6,192},{7,224},{32,1},... | collective-permute-start | bytes 786440 | tf_op jit(solution)/shard_map/ppermute | solution.py:27
  17.4 30.0 %copy-start = (bf16[1,256,4096]{1,2,0:T(8,128)(2,1)}, bf16[1,256,4096]{1,2,0:T(8,128)(2,1)S(1)}, u32[]{:S(2)}) copy-start(bf16[1,256,4096]{1,2,0:T(8,128)(2,1)S(1)} %copy.39) | copy-start | bytes 6291460
  32.6 0.7 copy-start.3
  51.5 33.0 %all-to-all-start.2 = ((bf16[32,256,128]{1,2,0:T(8,128)(2,1)}), bf16[32,256,128]{1,2,0:T(8,128)(2,1)}, u32[]{:S(2)}, u32[]{:S(2)}) async-start(bf16[32,256,128]{1,2,0:T(8,128)(2,1)} %bitcast.155), calls=%async_computation.2 | async-start | bytes 4194304 | tf_op jit(solution)/shard_map/all_to_all | solution.py:51
  102.5 33.5 %all-to-all-start.3 = ((bf16[32,256,128]{1,2,0:T(8,128)(2,1)}), bf16[32,256,128]{1,2,0:T(8,128)(2,1)}, u32[]{:S(2)}, u32[]{:S(2)}) async-start(bf16[32,256,128]{1,2,0:T(8,128)(2,1)} %copy.43), calls=%async_computation.3 | async-start | bytes 4194304 | tf_op jit(solution)/shard_map/all_to_all | solution.py:56
  119.4 16.6 %copy-start.4 = (f32[4096]{0:T(1024)S(1)}, f32[4096]{0:T(1024)}, u32[]{:S(2)}) copy-start(f32[4096]{0:T(1024)} %param.11) | copy-start | bytes 49156
  149.3 33.5 %all-to-all-start = ((bf16[32,256,128]{1,2,0:T(8,128)(2,1)}), bf16[32,256,128]{1,2,0:T(8,128)(2,1)}, u32[]{:S(2)}, u32[]{:S(2)}) async-start(bf16[32,256,128]{1,2,0:T(8,128)(2,1)} %fusion.121), calls=%async_computation | async-start | bytes 4194304 | tf_op jit(solution)/shard_map/all_to_all | solution.py:51
  156.8 174.8 %reduce-scatter.2.cloned.1.call-start = ((), (), s32[]{:S(2)}) async-start(), calls=%async_computation.6 | async-start | bytes 5308416 | tf_op jit(solution)/shard_map/reduce_scatter | solution.py:77
  193.9 0.7 copy-start.6
  194.6 9.8 %copy-start.2 = (bf16[32,256,128]{2,1,0:T(8,128)(2,1)S(1)}, bf16[32,256,128]{2,1,0:T(8,128)(2,1)}, u32[]{:S(2)}) copy-start(bf16[32,256,128]{2,1,0:T(8,128)(2,1)} %copy.35) | copy-start | bytes 6291460
  194.6 9.8 %copy-start.5 = (bf16[1024,1024]{1,0:T(8,128)(2,1)S(1)}, bf16[1024,1024]{1,0:T(8,128)(2,1)}, u32[]{:S(2)}) copy-start(bf16[1024,1024]{1,0:T(8,128)(2,1)} %all-gather.2.cloned.1.call-done) | copy-start | bytes 6291460
  194.6 9.8 %collective-permute-start.1 = (f32[1,1024]{1,0:T(1,128)S(1)}, f32[1,1024]{1,0:T(1,128)S(1)}, u32[]{:S(2)}, u32[]{:S(2)}) collective-permute-start(f32[1,1024]{1,0:T(1,128)S(1)} %copy-done.6), channel_id=1, source_target_pairs={{0,0},{1,32},{2,64},{3,96},{4,128},{5,160},{6,192},{7,224},{32,1},... | collective-permute-start | bytes 12296 | tf_op jit(solution)/shard_map/ppermute | solution.py:27
  212.0 105.0 %all-to-all-start.1 = ((bf16[32,256,128]{2,1,0:T(8,128)(2,1)}), bf16[32,256,128]{2,1,0:T(8,128)(2,1)}, u32[]{:S(2)}, u32[]{:S(2)}) async-start(bf16[32,256,128]{2,1,0:T(8,128)(2,1)} %bitcast.156), calls=%async_computation.1 | async-start | bytes 4194304 | tf_op jit(solution)/shard_map/all_to_all | solution.py:56
  326.8 8.7 %copy-start.1 = (bf16[1,256,4096]{1,2,0:T(8,128)(2,1)S(1)}, bf16[1,256,4096]{1,2,0:T(8,128)(2,1)}, u32[]{:S(2)}) copy-start(bf16[1,256,4096]{1,2,0:T(8,128)(2,1)} %copy-done) | copy-start | bytes 6291460
  331.6 45.7 %collective-permute-start.2 = (f32[128,1152]{0,1:T(8,128)}, f32[128,1152]{0,1:T(8,128)S(1)}, u32[]{:S(2)}, u32[]{:S(2)}) collective-permute-start(f32[128,1152]{0,1:T(8,128)} %reduce-scatter.2.cloned.1.call-done), channel_id=1, source_target_pairs={{0,0},{1,32},{2,64},{3,96},{4,128},{5,160},{6,192},{7,224},{32,1},... | collective-permute-start | bytes 1769480 | tf_op jit(solution)/shard_map/ppermute | solution.py:27
Sparse Core Ops, SparseCore 0:
  33.4 36.1 all-gather.1
  194.1 58.9 reduce-scatter.1
where the time goes:
time: 387 us; the launch traced here: 386 us
  waiting for transfers between devices  108 us (28%)
  other arithmetic  77.7 us (20%)
  blocking collectives  76.8 us (20%)
  local copies, waits for them, and re-layouts  47.5 us (12%)
  starting transfers between devices  47.3 us (12%)
  matrix products  14.2 us (4%)
  between operations  14.2 us (4%)
    psum x1, blocking collectives, shards(): gain_grad = lax.psum(jnp.sum(back_full * normed, axis=0), ALL)  76.8 us
    ppermute x3, waiting for transfers between devices, swapped(): return lax.ppermute(shard, SWAP, pairs)  48.7 us
    all_to_all x2, waiting for transfers between devices, outward(): got = lax.all_to_all(tok, PLANE, split_axis=0, concat_axis=0, tiled=True)  46.4 us
    unnamed x20, local copies, waits for them, and re-layouts  21.2 us
    ppermute x3, starting transfers between devices, swapped(): return lax.ppermute(shard, SWAP, pairs)  16.5 us
    all_to_all x2, starting transfers between devices, homeward(): got = lax.all_to_all(got, PLANE, split_axis=0, concat_axis=0, tiled=True)  16.1 us
    convert_element_type x1, other arithmetic, shards(): (value_slope * gelu_slope(value_arg)).astype(jnp.bfloat16)[None]  15.5 us
    all_to_all x2, starting transfers between devices, outward(): got = lax.all_to_all(tok, PLANE, split_axis=0, concat_axis=0, tiled=True)  14.5 us
  transfers between devices with their start and end apart: 9, of which 5 were waited for; matrix products, arithmetic and copies ran while one was open for 25% of the time, Pallas kernels for 0%

commit v1 on v0

--- a/solution.py
+++ b/solution.py
@@ -80,7 +80,9 @@
     bias_grad = both[None, :, block_len]
     up_mid = lax.optimization_barrier((grad_tok * mixed_tok).astype(jnp.bfloat16))
     up_grad = (up_mid.astype(jnp.float32) * gelu_slope(up_arg)).astype(jnp.bfloat16)[None]
-    gain_grad = lax.psum(jnp.sum(back_full * normed, axis=0), ALL)
+    a0 = jnp.sum(back_full * normed, axis=0)
+    u_next = lax.all_gather(a0, ALL)
+    gain_grad = jnp.sum(u_next, axis=0)
     scaled = back_full * value_gain
     value_slope = inv_rms * scaled - inv_rms**3 * value_act * jnp.mean(
         scaled * value_act, axis=-1, keepdims=True

time: 387 us -> 406 us (1.049)
  waiting for transfers between devices: 108 us -> 196 us
  blocking collectives: 76.8 us -> 0 us
  other arithmetic: 77.7 us -> 83.3 us
    all_gather x0 -> x1, waiting for transfers between devices: none -> 114 us  [shards(): u_next = lax.all_gather(a0, ALL)]
    psum x1 -> x0, blocking collectives: 76.8 us -> none  [shards(): gain_grad = lax.psum(jnp.sum(back_full * normed, axis=0), ALL)]
    ppermute x3, waiting for transfers between devices: 48.7 us -> 15.1 us  [swapped(): return lax.ppermute(shard, SWAP, pairs)]
    all_to_all x2, waiting for transfers between devices: 12.8 us -> 19.2 us  [homeward(): got = lax.all_to_all(got, PLANE, split_axis=0, concat_axis=0, tiled=True)]
    reduce_sum x1 -> x2, other arithmetic: 11.6 us -> 17.2 us  [the longest x1 12.2 us: shards(): a0 = jnp.sum(back_full * normed, axis=0)]
  transfers between devices with their start and end apart: 9 -> 10, of which waited for: 5 -> 6; matrix products, arithmetic and copies ran while one was open for 25% -> 26% of each run, Pallas kernels for 0% -> 0%
where the time goes in v1:
time: 406 us; the launch traced here: 401 us
  waiting for transfers between devices  196 us (48%)
  other arithmetic  83.3 us (21%)
  starting transfers between devices  47.1 us (12%)
  local copies, waits for them, and re-layouts  46.9 us (12%)
  matrix products  14.2 us (3%)
  between operations  13.9 us (3%)
    all_gather x1, waiting for transfers between devices, shards(): u_next = lax.all_gather(a0, ALL)  114 us
    all_to_all x2, waiting for transfers between devices, outward(): got = lax.all_to_all(tok, PLANE, split_axis=0, concat_axis=0, tiled=True)  46.4 us
    unnamed x20, local copies, waits for them, and re-layouts  20.5 us
    all_to_all x2, waiting for transfers between devices, homeward(): got = lax.all_to_all(got, PLANE, split_axis=0, concat_axis=0, tiled=True)  19.2 us
    ppermute x3, starting transfers between devices, swapped(): return lax.ppermute(shard, SWAP, pairs)  16.2 us
    all_to_all x2, starting transfers between devices, homeward(): got = lax.all_to_all(got, PLANE, split_axis=0, concat_axis=0, tiled=True)  16.1 us
    convert_element_type x1, other arithmetic, shards(): (value_slope * gelu_slope(value_arg)).astype(jnp.bfloat16)[None]  15.5 us
    ppermute x3, waiting for transfers between devices, swapped(): return lax.ppermute(shard, SWAP, pairs)  15.1 us
  transfers between devices with their start and end apart: 10, of which 6 were waited for; matrix products, arithmetic and copies ran while one was open for 26% of the time, Pallas kernels for 0%

profile of v1, /device:TPU:47, one launch (start us, length us, event | category | flops | bytes accessed | tf_op | source)
XLA Modules:
  0.0 401.4 jit_solution(1731284533966795312)
XLA Ops:
  7.2 6.9 %collective-permute-start = (bf16[128,1024]{1,0:T(8,128)(2,1)}, bf16[128,1024]{1,0:T(8,128)(2,1)S(1)}, u32[]{:S(2)}, u32[]{:S(2)}) collective-permute-start(bf16[128,1024]{1,0:T(8,128)(2,1)} %bitcast.165), channel_id=1, source_target_pairs={{0,0},{1,32},{2,64},{3,96},{4,128},{5,160},{6,192},{7,224},{32,1},... | collective-permute-start | bytes 786440 | tf_op jit(solution)/shard_map/ppermute | solution.py:27
  17.5 15.1 %collective-permute-done = bf16[128,1024]{1,0:T(8,128)(2,1)S(1)} collective-permute-done((bf16[128,1024]{1,0:T(8,128)(2,1)}, bf16[128,1024]{1,0:T(8,128)(2,1)S(1)}, u32[]{:S(2)}, u32[]{:S(2)}) %collective-permute-start) | collective-permute-done | bytes 262176 | tf_op jit(solution)/shard_map/ppermute | solution.py:27
  33.3 10.0 %fusion.10 = bf16[256,4096]{0,1:T(8,128)(2,1)} fusion(bf16[1,256,4096]{1,2,0:T(8,128)(2,1)S(1)} %copy.53), kind=kLoop, calls=%fused_computation.29 | loop fusion | flops 69206016 | bytes 4194304 | tf_op jit(solution)/shard_map/convert_element_type | solution.py:42
  43.3 4.1 %copy.47 = bf16[1,256,4096]{1,2,0:T(8,128)(2,1)} copy(bf16[1,256,4096]{2,1,0:T(8,128)(2,1)} %param.6) | data formatting | bytes 4194304 | tf_op args[0]
  47.4 4.1 %fusion.1 = bf16[256,4096]{0,1:T(8,128)(2,1)} fusion(bf16[256,4096]{0,1:T(8,128)(2,1)} %fusion.10, bf16[1,256,4096]{1,2,0:T(8,128)(2,1)} %copy.47), kind=kLoop, calls=%fused_computation.20 | loop fusion | flops 4194304 | bytes 6291456 | tf_op jit(solution)/shard_map/convert_element_type | solution.py:47
  51.5 7.0 %all-to-all-start.2 = ((bf16[32,256,128]{1,2,0:T(8,128)(2,1)}), bf16[32,256,128]{1,2,0:T(8,128)(2,1)}, u32[]{:S(2)}, u32[]{:S(2)}) async-start(bf16[32,256,128]{1,2,0:T(8,128)(2,1)} %bitcast.155), calls=%async_computation.2 | async-start | bytes 4194304 | tf_op jit(solution)/shard_map/all_to_all | solution.py:51
  61.8 22.7 %all-to-all-done.2 = bf16[32,256,128]{1,2,0:T(8,128)(2,1)} async-done(((bf16[32,256,128]{1,2,0:T(8,128)(2,1)}), bf16[32,256,128]{1,2,0:T(8,128)(2,1)}, u32[]{:S(2)}, u32[]{:S(2)}) %all-to-all-start.2) | async-done | bytes 2097184 | tf_op jit(solution)/shard_map/all_to_all | solution.py:51
  84.5 4.1 %copy.54 = bf16[32,256,128]{2,1,0:T(8,128)(2,1)} copy(bf16[32,256,128]{1,2,0:T(8,128)(2,1)} %all-to-all-done.2) | data formatting | bytes 4194304 | tf_op jit(solution)/shard_map/all_to_all | solution.py:51
  88.6 5.9 %convert_bitcast_fusion.1 = bf16[8,1024,128]{1,2,0:T(8,128)(2,1)} fusion(bf16[8,1024,128]{2,1,0:T(8,128)(2,1)} %bitcast.158, bf16[1024,1024]{1,0:T(8,128)(2,1)} %all-gather.4.cloned.1.call-done), kind=kOutput, calls=%fused_computation.165 | convolution fusion | flops 2148532224 | bytes 6291456 | tf_op jit(solution)/shard_map/pq,npc->nqc/dot_general | solution.py:61
  98.4 4.1 %copy.57 = bf16[32,256,128]{1,2,0:T(8,128)(2,1)} copy(bf16[32,256,128]{2,1,0:T(8,128)(2,1)} %bitcast.157) | data formatting | bytes 4194304 | tf_op jit(solution)/shard_map/reshape | solution.py:55
  102.5 7.5 %all-to-all-start.3 = ((bf16[32,256,128]{1,2,0:T(8,128)(2,1)}), bf16[32,256,128]{1,2,0:T(8,128)(2,1)}, u32[]{:S(2)}, u32[]{:S(2)}) async-start(bf16[32,256,128]{1,2,0:T(8,128)(2,1)} %copy.57), calls=%async_computation.3 | async-start | bytes 4194304 | tf_op jit(solution)/shard_map/all_to_all | solution.py:56
  110.0 9.4 %fusion.7 = f32[256]{0:T(256)S(1)} fusion(bf16[1,256,4096]{1,2,0:T(8,128)(2,1)S(1)} %copy.48), kind=kLoop, calls=%fused_computation.26 | loop fusion | flops 70254336 | bytes 2098176 | tf_op jit(solution)/shard_map/reduce_sum | solution.py:44
  123.2 12.8 %all-to-all-done.3 = bf16[32,256,128]{1,2,0:T(8,128)(2,1)} async-done(((bf16[32,256,128]{1,2,0:T(8,128)(2,1)}), bf16[32,256,128]{1,2,0:T(8,128)(2,1)}, u32[]{:S(2)}, u32[]{:S(2)}) %all-to-all-start.3) | async-done | bytes 2097184 | tf_op jit(solution)/shard_map/all_to_all | solution.py:56
  136.0 12.2 %fusion.61 = (f32[32,128]{1,0:T(8,128)}, f32[256]{0:T(256)S(1)}, f32[256,32,128]{0,2,1:T(8,128)S(1)}) fusion(bf16[32,256,128]{1,2,0:T(8,128)(2,1)} %all-to-all-done.3, f32[256]{0:T(256)S(1)} %get-tuple-element.36, f32[32,128]{1,0:T(8,128)S(1)} %bitcast.162, f32[256,32,128]{0,2,1:T(8,128)} %bitcast.154, f32[256,32,128]{0,2,1:T(8,128)} %bitcast.153), kind=kLoop, calls=%fused_computation.83 | loop fusion | flops 71298816 | bytes 14714880 | tf_op jit(solution)/shard_map/reduce_sum | solution.py:83
  149.9 7.5 %all-to-all-start = ((bf16[32,256,128]{1,2,0:T(8,128)(2,1)}), bf16[32,256,128]{1,2,0:T(8,128)(2,1)}, u32[]{:S(2)}, u32[]{:S(2)}) async-start(bf16[32,256,128]{1,2,0:T(8,128)(2,1)} %fusion.121), calls=%async_computation | async-start | bytes 4194304 | tf_op jit(solution)/shard_map/all_to_all | solution.py:51
  159.6 23.7 %all-to-all-done = bf16[32,256,128]{1,2,0:T(8,128)(2,1)} async-done(((bf16[32,256,128]{1,2,0:T(8,128)(2,1)}), bf16[32,256,128]{1,2,0:T(8,128)(2,1)}, u32[]{:S(2)}, u32[]{:S(2)}) %all-to-all-start) | async-done | bytes 2097184 | tf_op jit(solution)/shard_map/all_to_all | solution.py:51
  183.3 4.1 %copy.49 = bf16[32,256,128]{2,1,0:T(8,128)(2,1)} copy(bf16[32,256,128]{1,2,0:T(8,128)(2,1)} %all-to-all-done) | data formatting | bytes 4194304 | tf_op jit(solution)/shard_map/all_to_all | solution.py:51
  187.4 4.6 %convolution_bitcast_fusion = f32[1024,1024]{0,1:T(8,128)S(1)} fusion(bf16[8,1024,128]{2,1,0:T(8,128)(2,1)} %bitcast.159, bf16[8,1024,128]{2,1,0:T(8,128)(2,1)} %bitcast.160), kind=kOutput, calls=%fused_computation.158 | convolution fusion | flops 2147483648 | bytes 8388608 | tf_op jit(solution)/shard_map/npc,nqc->pq/dot_general | solution.py:70
  195.3 5.6 %collective-permute-start.1 = (f32[1,1024]{1,0:T(1,128)S(1)}, f32[1,1024]{1,0:T(1,128)S(1)}, u32[]{:S(2)}, u32[]{:S(2)}) collective-permute-start(f32[1,1024]{1,0:T(1,128)S(1)} %copy-done.6), channel_id=1, source_target_pairs={{0,0},{1,32},{2,64},{3,96},{4,128},{5,160},{6,192},{7,224},{32,1},... | collective-permute-start | bytes 12296 | tf_op jit(solution)/shard_map/ppermute | solution.py:27
  201.0 4.1 %convert_element_type.124 = f32[32,256,128]{1,2,0:T(8,128)} convert(bf16[32,256,128]{1,2,0:T(8,128)(2,1)} %all-to-all-done.3) | non-fusion elementwise | flops 1048576 | bytes 6291456 | tf_op jit(solution)/shard_map/convert_element_type | solution.py:64
  208.8 3.9 copy.51
  212.7 8.6 %all-to-all-start.1 = ((bf16[32,256,128]{2,1,0:T(8,128)(2,1)}), bf16[32,256,128]{2,1,0:T(8,128)(2,1)}, u32[]{:S(2)}, u32[]{:S(2)}) async-start(bf16[32,256,128]{2,1,0:T(8,128)(2,1)} %bitcast.156), calls=%async_computation.1 | async-start | bytes 4194304 | tf_op jit(solution)/shard_map/all_to_all | solution.py:56
  221.3 15.5 %fusion.17 = bf16[1,256,4096]{1,2,0:T(8,128)(2,1)} fusion(bf16[1,256,4096]{1,2,0:T(8,128)(2,1)S(1)} %copy.48, f32[256]{0:T(256)S(1)} %broadcast_multiply_fusion, f32[256]{0:T(256)S(1)} %get-tuple-element.35, f32[4096]{0:T(1024)S(1)} %copy-done.4, f32[256]{0:T(256)S(1)} %get-tuple-element.36, f32[1,256,4096]{1,2,0:T(8,128)} %bitcast.152), kind=kLoop, calls=%fused_computation.36 | loop fusion | flops 83886080 | bytes 8408064 | tf_op jit(solution)/shard_map/convert_element_type | solution.py:90
  236.9 4.1 %copy.59 = bf16[1,256,4096]{2,1,0:T(8,128)(2,1)} copy(bf16[1,256,4096]{1,2,0:T(8,128)(2,1)} %fusion.17) | data formatting | bytes 4194304
  240.9 6.4 %all-to-all-done.1 = bf16[32,256,128]{2,1,0:T(8,128)(2,1)} async-done(((bf16[32,256,128]{2,1,0:T(8,128)(2,1)}), bf16[32,256,128]{2,1,0:T(8,128)(2,1)}, u32[]{:S(2)}, u32[]{:S(2)}) %all-to-all-start.1) | async-done | bytes 2097184 | tf_op jit(solution)/shard_map/all_to_all | solution.py:56
  247.3 4.0 %convert_bitcast_fusion = f32[256,32,128]{2,0,1:T(8,128)} fusion(bf16[32,256,128]{2,1,0:T(8,128)(2,1)} %all-to-all-done.1), kind=kLoop, calls=%fused_computation.140 | loop fusion | flops 1048576 | bytes 6291456 | tf_op jit(solution)/shard_map/convert_element_type | solution.py:69
  251.3 5.7 %copy.52 = f32[256,32,128]{0,2,1:T(8,128)} copy(f32[256,32,128]{2,0,1:T(8,128)} %convert_bitcast_fusion) | data formatting | bytes 8388608 | tf_op jit(solution)/shard_map/convert_element_type | solution.py:69
  257.0 4.8 %fusion = bf16[256,4096]{0,1:T(8,128)(2,1)} fusion(f32[256,32,128]{0,2,1:T(8,128)} %copy.52, bf16[1,256,4096]{1,2,0:T(8,128)(2,1)} %copy.47), kind=kLoop, calls=%fused_computation.19 | loop fusion | flops 3145728 | bytes 8388608 | tf_op jit(solution)/shard_map/convert_element_type | solution.py:81
  265.5 4.2 %fusion.127 = bf16[1,256,4096]{1,2,0:T(8,128)(2,1)} fusion(bf16[1,256,4096]{1,2,0:T(8,128)(2,1)S(1)} %copy-done.1, bf16[256,4096]{0,1:T(8,128)(2,1)} %fusion), kind=kLoop, calls=%fused_computation.166 | loop fusion | flops 12582912 | bytes 6291456 | tf_op jit(solution)/shard_map/broadcast_in_dim | solution.py:82
  269.7 4.1 %copy.58 = bf16[1,256,4096]{2,1,0:T(8,128)(2,1)} copy(bf16[1,256,4096]{1,2,0:T(8,128)(2,1)} %fusion.127) | data formatting | bytes 4194304
  273.8 114.4 %all-gather.6.cloned.1.call-done = f32[256,1,4096]{2,1,0:T(1,128)} async-done(((f32[1,1,4096]{2,1,0:T(1,128)}), f32[256,1,4096]{2,1,0:T(1,128)}) %all-gather.6.cloned.1.call-update) | async-done | bytes 4194320 | tf_op jit(solution)/shard_map/all_gather | solution.py:84
  388.2 5.1 %reduce_sum.58 = f32[4096]{0:T(1024)} reduce(f32[256,1,4096]{2,1,0:T(1,128)} %all-gather.6.cloned.1.call-done, f32[]{:T(128)} %constant.10.clone.1), dimensions={0,1}, to_apply=%region_6.7 | reduce | flops 1044480 | bytes 4210692 | tf_op jit(solution)/shard_map/reduce_sum | solution.py:85
  (41 shorter events, 31.2 us)
Async XLA Ops:
  7.2 81.4 %all-gather.4.cloned.1.call-start = ((), (), s32[]{:S(2)}) async-start(), calls=%async_computation.5 | async-start | bytes 2359296 | tf_op jit(solution)/shard_map/all_gather | solution.py:37
  7.2 25.4 %collective-permute-start = (bf16[128,1024]{1,0:T(8,128)(2,1)}, bf16[128,1024]{1,0:T(8,128)(2,1)S(1)}, u32[]{:S(2)}, u32[]{:S(2)}) collective-permute-start(bf16[128,1024]{1,0:T(8,128)(2,1)} %bitcast.165), channel_id=1, source_target_pairs={{0,0},{1,32},{2,64},{3,96},{4,128},{5,160},{6,192},{7,224},{32,1},... | collective-permute-start | bytes 786440 | tf_op jit(solution)/shard_map/ppermute | solution.py:27
  17.4 29.9 %copy-start = (bf16[1,256,4096]{1,2,0:T(8,128)(2,1)}, bf16[1,256,4096]{1,2,0:T(8,128)(2,1)S(1)}, u32[]{:S(2)}) copy-start(bf16[1,256,4096]{1,2,0:T(8,128)(2,1)S(1)} %copy.53) | copy-start | bytes 6291460
  32.6 0.7 copy-start.3
  51.5 33.0 %all-to-all-start.2 = ((bf16[32,256,128]{1,2,0:T(8,128)(2,1)}), bf16[32,256,128]{1,2,0:T(8,128)(2,1)}, u32[]{:S(2)}, u32[]{:S(2)}) async-start(bf16[32,256,128]{1,2,0:T(8,128)(2,1)} %bitcast.155), calls=%async_computation.2 | async-start | bytes 4194304 | tf_op jit(solution)/shard_map/all_to_all | solution.py:51
  102.5 33.5 %all-to-all-start.3 = ((bf16[32,256,128]{1,2,0:T(8,128)(2,1)}), bf16[32,256,128]{1,2,0:T(8,128)(2,1)}, u32[]{:S(2)}, u32[]{:S(2)}) async-start(bf16[32,256,128]{1,2,0:T(8,128)(2,1)} %copy.57), calls=%async_computation.3 | async-start | bytes 4194304 | tf_op jit(solution)/shard_map/all_to_all | solution.py:56
  119.4 16.6 %copy-start.4 = (f32[4096]{0:T(1024)S(1)}, f32[4096]{0:T(1024)}, u32[]{:S(2)}) copy-start(f32[4096]{0:T(1024)} %param.11) | copy-start | bytes 49156
  149.9 33.5 %all-to-all-start = ((bf16[32,256,128]{1,2,0:T(8,128)(2,1)}), bf16[32,256,128]{1,2,0:T(8,128)(2,1)}, u32[]{:S(2)}, u32[]{:S(2)}) async-start(bf16[32,256,128]{1,2,0:T(8,128)(2,1)} %fusion.121), calls=%async_computation | async-start | bytes 4194304 | tf_op jit(solution)/shard_map/all_to_all | solution.py:51
  157.4 104.5 %reduce-scatter.2.cloned.1.call-start = ((), (), s32[]{:S(2)}) async-start(), calls=%async_computation.6 | async-start | bytes 5308416 | tf_op jit(solution)/shard_map/reduce_scatter | solution.py:77
  194.5 0.8 copy-start.6
  194.6 193.6 %all-gather.6.cloned.1.call-start = ((), (), s32[]{:S(2)}) async-start(), calls=%async_computation.7 | async-start | bytes 4210688 | tf_op jit(solution)/shard_map/all_gather | solution.py:84
  195.3 9.8 %copy-start.2 = (bf16[32,256,128]{2,1,0:T(8,128)(2,1)S(1)}, bf16[32,256,128]{2,1,0:T(8,128)(2,1)}, u32[]{:S(2)}) copy-start(bf16[32,256,128]{2,1,0:T(8,128)(2,1)} %copy.49) | copy-start | bytes 6291460
  195.3 9.8 %copy-start.5 = (bf16[1024,1024]{1,0:T(8,128)(2,1)S(1)}, bf16[1024,1024]{1,0:T(8,128)(2,1)}, u32[]{:S(2)}) copy-start(bf16[1024,1024]{1,0:T(8,128)(2,1)} %all-gather.4.cloned.1.call-done) | copy-start | bytes 6291460
  195.3 9.8 %collective-permute-start.1 = (f32[1,1024]{1,0:T(1,128)S(1)}, f32[1,1024]{1,0:T(1,128)S(1)}, u32[]{:S(2)}, u32[]{:S(2)}) collective-permute-start(f32[1,1024]{1,0:T(1,128)S(1)} %copy-done.6), channel_id=1, source_target_pairs={{0,0},{1,32},{2,64},{3,96},{4,128},{5,160},{6,192},{7,224},{32,1},... | collective-permute-start | bytes 12296 | tf_op jit(solution)/shard_map/ppermute | solution.py:27
  212.7 34.5 %all-to-all-start.1 = ((bf16[32,256,128]{2,1,0:T(8,128)(2,1)}), bf16[32,256,128]{2,1,0:T(8,128)(2,1)}, u32[]{:S(2)}, u32[]{:S(2)}) async-start(bf16[32,256,128]{2,1,0:T(8,128)(2,1)} %bitcast.156), calls=%async_computation.1 | async-start | bytes 4194304 | tf_op jit(solution)/shard_map/all_to_all | solution.py:56
  257.0 8.5 %copy-start.1 = (bf16[1,256,4096]{1,2,0:T(8,128)(2,1)S(1)}, bf16[1,256,4096]{1,2,0:T(8,128)(2,1)}, u32[]{:S(2)}) copy-start(bf16[1,256,4096]{1,2,0:T(8,128)(2,1)} %copy-done) | copy-start | bytes 6291460
  261.8 131.5 %collective-permute-start.2 = (f32[128,1152]{0,1:T(8,128)}, f32[128,1152]{0,1:T(8,128)S(1)}, u32[]{:S(2)}, u32[]{:S(2)}) collective-permute-start(f32[128,1152]{0,1:T(8,128)} %reduce-scatter.2.cloned.1.call-done), channel_id=1, source_target_pairs={{0,0},{1,32},{2,64},{3,96},{4,128},{5,160},{6,192},{7,224},{32,1},... | collective-permute-start | bytes 1769480 | tf_op jit(solution)/shard_map/ppermute | solution.py:27
Sparse Core Ops, SparseCore 0:
  33.4 36.1 all-gather.3
  194.7 58.9 reduce-scatter.1
  257.9 130.2 all-gather.5
